TPU v7x, 32 devices: a whole 2x2x4 slice. The times are simulated.
32 devices in a mesh: sp: 8 (over z, x), tp: 4 (over y, core).
Axes of the slice: x: 2, y: 2, z: 4, core: 2. Of those that a mesh axis runs over, the one named last changes fastest.
Arguments:
- tokens: bfloat16 [8192, 2048], P('sp', 'tp'), may hold values from -70 to 70
- w_query: bfloat16 [2048, 1024], P(None, 'tp'), may hold values from -0.125 to 0.125
- w_key: bfloat16 [2048, 1024], P(None, 'tp'), may hold values from -0.125 to 0.125
- w_value: bfloat16 [2048, 1024], P(None, 'tp'), may hold values from -0.125 to 0.125
- w_delta_gate: bfloat16 [2048, 1024], P(None, 'tp'), may hold values from -0.125 to 0.125
- w_glu_value: bfloat16 [2048, 1024], P(None, 'tp'), may hold values from -0.125 to 0.125
- w_glu_gate: bfloat16 [2048, 1024], P(None, 'tp'), may hold values from -0.125 to 0.125
- w_conv_gate: bfloat16 [2048, 1024], P(None, 'tp'), may hold values from -0.125 to 0.125
- w_beta: bfloat16 [2048, 8], replicated, may hold values from -0.125 to 0.125
- w_decay: bfloat16 [2048, 8], replicated, may hold values from -0.125 to 0.125
- decay_log: float32 [8], replicated, may hold values from -12 to -3
- head_gain: float32 [128], replicated, may hold values from 0.1 to 1.9
- conv_taps: bfloat16 [31, 1024], P(None, 'tp'), may hold values from -2.5 to 2.5
- ln_gain: float32 [1024], P('tp'), may hold values from 0.1 to 1.9
- ln_shift: float32 [1024], P('tp'), may hold values from -3 to 3
- out_delta: bfloat16 [1024, 2048], P('tp'), may hold values from -0.125 to 0.125
- out_conv: bfloat16 [1024, 2048], P('tp'), may hold values from -0.125 to 0.125
Outputs:
- mixed_out: bfloat16 [8192, 2048], P(('sp', 'tp'))
All inputs are finite; a program needn't handle non-finite values.
Results may differ from a plain program's by a relative error of at most 0.024.
Values may be sent and summed in bfloat16 or wider, within the bound.
A program may use at most 64 MiB of HBM per device.

v0:
```python
import jax
import jax.numpy as jnp
from jax import lax
from jax.sharding import PartitionSpec as P

SPAN = 64
TINY_NORM = 1e-06
TINY_VAR = 1e-05
HIGHEST = lax.Precision.HIGHEST


def entering(part, axis, combine, identity):
    place = lax.axis_index(axis)
    gathered = lax.all_gather(part, axis)
    state = jnp.zeros_like(part) + jnp.asarray(identity, part.dtype)

    def one(hop, state):
        return combine(state, lax.dynamic_index_in_dim(gathered, hop, 0, False))

    return lax.fori_loop(0, place, one, state)


def shifted(block, axis, distance):
    devices = range(lax.axis_size(axis))
    route = [(i - distance, i) for i in devices if i - distance in devices]
    return lax.ppermute(block, axis, route)


def block_terms(query, keys, values, strength, log_decay):
    log_sum = jnp.cumsum(log_decay, axis=-1)
    offsets = jnp.arange(SPAN)
    causal = offsets[:, None] >= offsets[None, :]
    strict = offsets[:, None] > offsets[None, :]
    spread = log_sum[..., :, None] - log_sum[..., None, :]
    damping = jnp.where(causal, jnp.exp(jnp.where(causal, spread, 0.0)), 0.0)
    scaled_keys = keys * strength[..., None]
    lower = jnp.where(
        strict, jnp.einsum("hnid,hnjd->hnij", scaled_keys, keys, precision=HIGHEST) * damping, 0.0
    )
    identity = jnp.eye(SPAN, dtype=jnp.float32)
    right = jnp.concatenate(
        [values * strength[..., None], scaled_keys * jnp.exp(log_sum)[..., None]], axis=-1
    )
    solved = jax.scipy.linalg.solve_triangular(
        identity + lower, right, lower=True, unit_diagonal=True
    )
    width = values.shape[-1]
    scores = jnp.einsum("hnid,hnjd->hnij", query, keys, precision=HIGHEST) * damping
    return (log_sum, solved[..., :width], solved[..., width:], scores)


def local(
    tokens,
    w_query,
    w_key,
    w_value,
    w_delta_gate,
    w_glu_value,
    w_glu_gate,
    w_conv_gate,
    w_beta,
    w_decay,
    decay_log,
    head_gain,
    conv_taps,
    ln_gain,
    ln_shift,
    out_delta,
    out_conv,
):
    rows_here = tokens.shape[0]
    tp_size = lax.axis_size("tp")
    width_all = tokens.shape[1] * tp_size
    weights = (
        w_query,
        w_key,
        w_value,
        w_delta_gate,
        w_glu_value,
        w_glu_gate,
        w_conv_gate,
        w_beta,
        w_decay,
    )
    piece = lax.all_gather(tokens, "tp", axis=1, tiled=True)
    totals = tuple(
        (jnp.dot(piece, weight, preferred_element_type=jnp.float32) for weight in weights)
    )
    squares = jnp.sum(jnp.square(piece.astype(jnp.float32)), axis=1)
    sums, squares = (totals, squares)
    inv_rms = lax.rsqrt(squares / width_all + TINY_NORM)[:, None]
    scaled = [summed * inv_rms for summed in sums]
    query_raw, key_raw, value_raw, delta_gate_raw, glu_value_raw, glu_gate_raw, conv_gate_raw = [
        item.astype(jnp.bfloat16) for item in scaled[:7]
    ]
    head_size = head_gain.shape[0]
    heads_here = w_query.shape[1] // head_size
    first_head = lax.axis_index("tp") * heads_here
    strength = jax.nn.sigmoid(lax.dynamic_slice_in_dim(scaled[7], first_head, heads_here, 1))
    rates = jnp.exp(lax.dynamic_slice_in_dim(decay_log, first_head, heads_here, 0))
    log_decay = -rates[None, :] * jax.nn.softplus(
        lax.dynamic_slice_in_dim(scaled[8], first_head, heads_here, 1)
    )
    blocks = rows_here // SPAN

    def to_blocks(raw):
        return jnp.transpose(raw.reshape(blocks, SPAN, heads_here, head_size), (2, 0, 1, 3))

    def unit_rows(array):
        return array * lax.rsqrt(jnp.sum(array * array, axis=-1, keepdims=True) + TINY_NORM)

    query = unit_rows(to_blocks(query_raw.astype(jnp.float32))) * head_size ** (-0.5)
    keys = unit_rows(to_blocks(key_raw.astype(jnp.float32)))
    values = to_blocks(value_raw.astype(jnp.float32))
    strength_blocks = jnp.transpose(strength.reshape(blocks, SPAN, heads_here), (2, 0, 1))
    decay_blocks = jnp.transpose(log_decay.reshape(blocks, SPAN, heads_here), (2, 0, 1))
    log_sum, corrected, key_terms, scores = block_terms(
        query, keys, values, strength_blocks, decay_blocks
    )

    def advance(memory, inputs):
        query_block, keys_block, corrected_block, terms_block, scores_block, log_block = inputs
        extended = jnp.concatenate([jnp.zeros_like(corrected_block), corrected_block], axis=-1)
        fresh = extended - jnp.einsum("hcd,hde->hce", terms_block, memory, precision=HIGHEST)
        output = jnp.einsum(
            "hcd,hde->hce", query_block * jnp.exp(log_block)[..., None], memory, precision=HIGHEST
        )
        output = output + jnp.einsum("hcs,hse->hce", scores_block, fresh, precision=HIGHEST)
        tail_log = log_block[:, -1:]
        weighted = keys_block * jnp.exp(tail_log - log_block)[..., None]
        memory = memory * jnp.exp(tail_log)[..., None] + jnp.einsum(
            "hcd,hce->hde", weighted, fresh, precision=HIGHEST
        )
        return (memory, output)

    start_state = jnp.concatenate(
        [
            jnp.broadcast_to(
                jnp.eye(head_size, dtype=jnp.float32), (heads_here, head_size, head_size)
            ),
            jnp.zeros((heads_here, head_size, head_size), jnp.float32),
        ],
        axis=-1,
    )
    sequence_inputs = tuple(
        (jnp.moveaxis(item, 1, 0) for item in (query, keys, corrected, key_terms, scores, log_sum))
    )
    final, outputs = lax.scan(advance, start_state, sequence_inputs)
    outputs = jnp.moveaxis(outputs, 0, 1).reshape(heads_here, rows_here, 2 * head_size)

    def compose(earlier, later):
        moved = jnp.einsum("hij,hjk->hik", later[..., :head_size], earlier, precision=HIGHEST)
        return moved + jnp.concatenate(
            [jnp.zeros_like(later[..., :head_size]), later[..., head_size:]], axis=-1
        )

    prefix = entering(final, "sp", compose, start_state)
    carried = prefix[..., head_size:]
    result = outputs[..., head_size:] + jnp.einsum(
        "htd,hde->hte", outputs[..., :head_size], carried, precision=HIGHEST
    )
    result = jnp.transpose(result, (1, 0, 2))
    result = (
        result
        * lax.rsqrt(jnp.mean(result * result, axis=-1, keepdims=True) + TINY_NORM)
        * head_gain
    )
    delta_mixed = (
        result.reshape(rows_here, heads_here * head_size)
        * jax.nn.silu(delta_gate_raw.astype(jnp.float32))
    ).astype(jnp.bfloat16)
    kernel = conv_taps.shape[0]
    channels = conv_taps.shape[1]
    gated_units = (
        glu_value_raw.astype(jnp.float32) * jax.nn.sigmoid(glu_gate_raw.astype(jnp.float32))
    ).astype(jnp.bfloat16)
    before = shifted(gated_units[rows_here - (kernel - 1) :], "sp", 1)
    padded = jnp.concatenate([before, gated_units], axis=0)
    filtered = jnp.zeros((rows_here, channels), jnp.float32)
    for offset in range(kernel):
        filtered = filtered + padded[offset : offset + rows_here].astype(jnp.float32) * conv_taps[
            offset
        ].astype(jnp.float32)
    first_sum = jnp.sum(filtered, axis=1)
    second_sum = jnp.sum(filtered * filtered, axis=1)
    first_sum, second_sum = lax.psum((first_sum, second_sum), "tp")
    channels_all = channels * tp_size
    center = first_sum / channels_all
    variance = jnp.maximum(second_sum / channels_all - center * center, 0.0)
    normed = (filtered - center[:, None]) * lax.rsqrt(variance + TINY_VAR)[
        :, None
    ] * ln_gain + ln_shift
    conv_mixed = (jax.nn.silu(normed) * jax.nn.silu(conv_gate_raw.astype(jnp.float32))).astype(
        jnp.bfloat16
    )
    summed = jnp.dot(delta_mixed, out_delta, preferred_element_type=jnp.float32)
    return lax.psum_scatter(
        (summed + jnp.dot(conv_mixed, out_conv, preferred_element_type=jnp.float32)).astype(
            jnp.bfloat16
        ),
        "tp",
        scatter_dimension=0,
        tiled=True,
    )


def solution(mesh):
    return jax.shard_map(
        local,
        mesh=mesh,
        in_specs=(
            P("sp", "tp"),
            P(None, "tp"),
            P(None, "tp"),
            P(None, "tp"),
            P(None, "tp"),
            P(None, "tp"),
            P(None, "tp"),
            P(None, "tp"),
            P(),
            P(),
            P(),
            P(),
            P(None, "tp"),
            P("tp"),
            P("tp"),
            P("tp", None),
            P("tp", None),
        ),
        out_specs=P(("sp", "tp"), None),
        check_vma=False,
    )
```

profile of v0, /device:TPU:0, one launch (start us, length us, event | category | flops | bytes accessed | tf_op | source)
XLA Modules:
  0.0 483.8 jit_solution(3299517887842109902)
XLA Ops:
  9.5 36.6 %all-gather.4.cloned.1.call-done = bf16[1024,2048]{1,0:T(8,128)(2,1)} async-done(((bf16[1024,512]{1,0:T(8,128)(2,1)}), bf16[1024,2048]{1,0:T(8,128)(2,1)}) %all-gather.4.cloned.1.call-update) | async-done | bytes 4194320 | tf_op jit(solution)/shard_map/all_gather | solution.py:85
  46.1 3.2 multiply_reduce_fusion
  52.8 3.4 fusion.45
  57.8 3.7 fusion.47
  62.4 4.7 fusion.43
  69.9 3.8 fusion.39
  73.7 158.7 %custom-call.4 = f32[2,16,1,64,64]{3,4,2,1,0:T(8,128)} custom-call(f32[2,16,1,64,64]{4,3,2,1,0:T(8,128)} %fusion.39), custom_call_target="InvertDiagBlocksLowerTriangular" | custom-call | tf_op jit(solution)/shard_map/jit(_solve_triangular)/vmap(vmap())/triangular_solve | solution.py:44
  232.4 2.1 bitcast_multiply_fusion.7
  234.5 2.0 fusion.16
  240.8 3.1 fusion.26
  243.9 104.2 %while.22 = (s32[]{:T(128)}, f32[2,128,256]{2,1,0:T(8,128)S(1)}, f32[16,2,64,256]{3,2,1,0:T(8,128)}, f32[16,2,64]{2,0,1:T(8,128)S(1)}, f32[16,2,64,128]{3,2,1,0:...) while((s32[]{:T(128)}, f32[2,128,256]{2,1,0:T(8,128)S(1)}, ...), condition=%wide.region_5.6_spmd, body=%wide.region_4.5_spmd.sunk | while | flops 176390272 | bytes 2298537 | solution.py:148
  261.7 1.8 fusion.190
  281.3 1.8 fusion.190
  326.9 1.8 fusion.190
  349.0 3.6 fusion.58
  354.8 3.5 collective-permute-start
  358.9 1.8 copy.62
  360.8 6.0 %fusion.142 = (f32[1024]{0:T(1024)S(1)}, f32[1024]{0:T(1024)S(1)}, f32[1024,256]{1,0:T(8,128)}) fusion(f32[256]{0:T(256)S(1)} %bitcast.215, bf16[1024,256]{1,0:T(8,128)(2,1)S(1)} %copy-done.10, f32[256]{0:T(256)S(1)} %bitcast.216, bf16[30,256]{1,0:T(8,128)(2,1)S(1)} %collective-permute-done, f32[256]{0:T(256)S(1)} %bitcast.187, f32[256]{0:T(256)S(1)} %bitcast.188, ...), kind=kLoop, calls=%fused_computation.252 | loop fusion | flops 48494592 | bytes 1628160 | tf_op jit(solution)/shard_map/reduce_sum | solution.py:184
  366.8 6.3 %all-reduce.3 = (f32[1024]{0:T(1024)S(1)}, f32[1024]{0:T(1024)S(1)}) all-reduce(f32[1024]{0:T(1024)S(1)} %get-tuple-element.109, f32[1024]{0:T(1024)S(1)} %get-tuple-element.108), channel_id=1, replica_groups=mesh['sp'=8,'tp'=4] {'tp'}, use_global_device_ids=true, to_apply=%region_12.13 | all-reduce | flops 2048 | bytes 16384 | tf_op jit(solution)/shard_map/psum | solution.py:186
  373.1 25.1 %all-gather.6.cloned.1.call-done = f32[16,128,256]{2,1,0:T(8,128)} async-done(((f32[2,128,256]{2,1,0:T(8,128)}), f32[16,128,256]{2,1,0:T(8,128)}) %all-gather.6.cloned.1.call-update) | async-done | bytes 2097168 | tf_op jit(solution)/shard_map/all_gather | solution.py:14
  399.0 2.9 multiply_reduce_fusion.2
  402.0 10.6 %fusion.65 = f32[1024,2048]{1,0:T(8,128)} fusion(bf16[256,2048]{1,0:T(8,128)(2,1)S(1)} %copy-done, bf16[1024,2048]{1,0:T(8,128)(2,1)} %all-gather.4.cloned.1.call-done, bf16[2048,256]{1,0:T(8,128)(2,1)} %param.25, f32[1024]{0:T(1024)S(1)} %add_rsqrt_fusion.4, f32[1024,2,128]{2,0,1:T(8,128)} %get-tuple-element.185, f32[128]{0:T(128)S(1)} %copy-done.22, ...), kind=kOutput, calls=%fused_computation.110 | convolution fusion | flops 2150367232 | bytes 15741440 | tf_op jit(solution)/shard_map/dot_general | solution.py:196
  412.6 11.5 %add_convert_fusion = bf16[1024,2048]{1,0:T(8,128)(2,1)} fusion(f32[1024,2048]{1,0:T(8,128)} %fusion.65, bf16[256,2048]{1,0:T(8,128)(2,1)S(1)} %copy-done.26, bf16[1024,2048]{1,0:T(8,128)(2,1)} %all-gather.4.cloned.1.call-done, bf16[2048,256]{1,0:T(8,128)(2,1)} %param.28, f32[1024,256]{1,0:T(8,128)S(1)} %copy-done.8, f32[256]{0:T(256)S(1)} %copy-done.27, ...), kind=kOutput, calls=%fused_computation.28 | convolution fusion | flops 2156134400 | bytes 19937280 | tf_op jit(solution)/shard_map/dot_general | solution.py:198
  424.2 53.2 %reduce-scatter.2.cloned.1.call-done = bf16[256,2048]{1,0:T(8,128)(2,1)} async-done(((bf16[1024,2048]{1,0:T(8,128)(2,1)}), bf16[256,2048]{1,0:T(8,128)(2,1)}) %reduce-scatter.2.cloned.1.call-update) | async-done | bytes 1048592 | tf_op jit(solution)/shard_map/reduce_scatter | solution.py:197
  (226 shorter events, 118.6 us)
Async XLA Ops:
  6.5 395.4 %copy-start = (bf16[256,2048]{1,0:T(8,128)(2,1)S(1)}, bf16[256,2048]{1,0:T(8,128)(2,1)}, u32[]{:S(2)}) copy-start(bf16[256,2048]{1,0:T(8,128)(2,1)} %param.36) | copy-start | bytes 3145732
  6.5 42.8 %copy-start.13 = (bf16[2048,8]{0,1:T(8,128)(2,1)S(1)}, bf16[2048,8]{0,1:T(8,128)(2,1)}, u32[]{:S(2)}) copy-start(bf16[2048,8]{0,1:T(8,128)(2,1)} %param.29) | copy-start | bytes 98308
  6.5 39.6 %all-gather.4.cloned.1.call-start = ((), (), s32[]{:S(2)}) async-start(), calls=%async_computation.1 | async-start | bytes 5242880 | tf_op jit(solution)/shard_map/all_gather | solution.py:85
  7.3 390.9 %all-gather.6.cloned.1.call-start = ((), (), s32[]{:S(2)}) async-start(), calls=%async_computation.3 | async-start | bytes 2359296 | tf_op jit(solution)/shard_map/all_gather | solution.py:14
  7.4 50.4 %copy-start.3 = (f32[2,128,256]{2,1,0:T(8,128)}, f32[2,128,256]{2,1,0:T(8,128)S(1)}, u32[]{:S(2)}) copy-start(f32[2,128,256]{2,1,0:T(8,128)S(1)} %concatenate.15) | copy-start | bytes 786436
  46.1 3.4 copy-start.1
  46.1 4.6 copy-start.14
  62.4 7.5 %copy-start.12 = (f32[64,64]{1,0:T(8,128)S(1)}, f32[64,64]{1,0:T(8,128)}, u32[]{:S(2)}) copy-start(f32[64,64]{1,0:T(8,128)} %get-tuple-element.189) | copy-start | bytes 49156
  62.4 7.5 %copy-start.16 = (pred[64,64]{1,0:T(8,128)(4,1)S(1)}, pred[64,64]{1,0:T(8,128)(4,1)}, u32[]{:S(2)}) copy-start(pred[64,64]{1,0:T(8,128)(4,1)} %get-tuple-element.187) | copy-start | bytes 12292
  62.4 7.5 %copy-start.17 = (pred[64,64]{1,0:T(8,128)(4,1)S(1)}, pred[64,64]{1,0:T(8,128)(4,1)}, u32[]{:S(2)}) copy-start(pred[64,64]{1,0:T(8,128)(4,1)} %get-tuple-element.188) | copy-start | bytes 12292
  236.5 4.3 copy-start.15
  238.1 5.8 %copy-start.6 = (f32[2,128,256]{2,1,0:T(8,128)S(1)}, f32[2,128,256]{2,1,0:T(8,128)}, u32[]{:S(2)}) copy-start(f32[2,128,256]{2,1,0:T(8,128)} %copy-done.3) | copy-start | bytes 786436
  243.9 105.0 %copy-start.11 = (bf16[31,256]{1,0:T(8,128)(2,1)S(1)}, bf16[31,256]{1,0:T(8,128)(2,1)}, u32[]{:S(2)}) copy-start(bf16[31,256]{1,0:T(8,128)(2,1)} %param.33) | copy-start | bytes 47620
  243.9 105.1 %copy-start.24 = (bf16[2048,256]{1,0:T(8,128)(2,1)S(1)}, bf16[2048,256]{1,0:T(8,128)(2,1)}, u32[]{:S(2)}) copy-start(bf16[2048,256]{1,0:T(8,128)(2,1)} %param.27) | copy-start | bytes 3145732
  348.9 128.4 %reduce-scatter.2.cloned.1.call-start = ((), (), s32[]{:S(2)}) async-start(), calls=%async_computation.2 | async-start | bytes 5242880 | tf_op jit(solution)/shard_map/reduce_scatter | solution.py:197
  349.0 3.7 copy-start.2
  349.0 3.7 copy-start.25
  354.8 43.4 %copy-start.4 = (f32[2,128,256]{2,1,0:T(8,128)S(1)}, f32[2,128,256]{2,1,0:T(8,128)}, u32[]{:S(2)}) copy-start(f32[2,128,256]{2,1,0:T(8,128)} %copy-done.3) | copy-start | bytes 786436
  354.8 5.9 %collective-permute-start = (bf16[30,256]{1,0:T(8,128)(2,1)S(1)}, bf16[30,256]{1,0:T(8,128)(2,1)S(1)}, u32[]{:S(2)}, u32[]{:S(2)}) collective-permute-start(bf16[30,256]{1,0:T(8,128)(2,1)S(1)} %slice.292), channel_id=1, source_target_pairs={{0,4},{4,8},{8,12},{12,16},{16,20},{20,24},{24,28},{1,5},{5,9},{9,... | collective-permute-start | bytes 46088 | tf_op jit(solution)/shard_map/ppermute | solution.py:26
  398.2 3.8 copy-start.22
  401.9 10.6 %copy-start.8 = (f32[1024,256]{1,0:T(8,128)S(1)}, f32[1024,256]{1,0:T(8,128)}, u32[]{:S(2)}) copy-start(f32[1024,256]{1,0:T(8,128)} %get-tuple-element.138) | copy-start | bytes 3145732
  402.0 10.6 %copy-start.26 = (bf16[256,2048]{1,0:T(8,128)(2,1)S(1)}, bf16[256,2048]{1,0:T(8,128)(2,1)}, u32[]{:S(2)}) copy-start(bf16[256,2048]{1,0:T(8,128)(2,1)} %param.37) | copy-start | bytes 3145732
  402.0 10.6 %copy-start.27 = (f32[256]{0:T(256)S(1)}, f32[256]{0:T(256)}, u32[]{:S(2)}) copy-start(f32[256]{0:T(256)} %param.35) | copy-start | bytes 3076
  402.0 10.6 %copy-start.28 = (f32[256]{0:T(256)S(1)}, f32[256]{0:T(256)}, u32[]{:S(2)}) copy-start(f32[256]{0:T(256)} %param.34) | copy-start | bytes 3076
  (9 other events, 16.2 us)
Sparse Core Ops, SparseCore 0:
  8.9 37.1 all-gather.3
  349.0 49.1 all-gather.5
  424.3 52.9 reduce-scatter.1
where the time goes:
time: 488 us; the launch traced here: 484 us
  other arithmetic  178 us (36%)
  matrix products  139 us (28%)
  waiting for transfers between devices  116 us (24%)
  local copies, waits for them, and re-layouts  27.1 us (6%)
  between operations  13.6 us (3%)
  blocking collectives  6.3 us (1%)
    another operation x4, other arithmetic, block_terms(): jax.scipy.linalg.solve_triangular(identity + lower, right, lower=True, un...  159 us
    reduce_scatter x1, waiting for transfers between devices, local(): lax.psum_scatter((summed + jnp.dot(conv_mixed, out_conv, preferred_elemen...  53.2 us
    all_gather x1, waiting for transfers between devices, local(): piece = lax.all_gather(tokens, 'tp', axis=1, tiled=True)  36.6 us
    dot_general x16, matrix products, advance(): jnp.einsum('hcs,hse->hce', scores_block, fresh, precision=HIGHEST)  28.1 us
    all_gather x1, waiting for transfers between devices, entering(): gathered = lax.all_gather(part, axis)  25.1 us
    dot_general x16, matrix products, advance(): jnp.einsum('hcd,hce->hde', weighted, fresh, precision=HIGHEST)  21.5 us
    dot_general x7, matrix products, local(): jnp.dot(piece, weight, preferred_element_type=jnp.float32)  19.2 us
    dot_general x16, matrix products, advance(): jnp.einsum('hcd,hde->hce', query_block * jnp.exp(log_block)[..., None], m...  18.5 us
  transfers between devices with their start and end apart: 4, of which 3 were waited for; matrix products, arithmetic and copies ran while one was open for 3% of the time, Pallas kernels for 0%

commit v1 on v0

--- a/solution.py
+++ b/solution.py
@@ -7,6 +7,12 @@
 TINY_NORM = 1e-06
 TINY_VAR = 1e-05
 HIGHEST = lax.Precision.HIGHEST
+
+
+def laid_out(tiles, dim):
+    shape = list(tiles.shape[1:])
+    shape[dim] *= tiles.shape[0]
+    return jnp.moveaxis(tiles, 0, dim).reshape(shape)
 
 
 def entering(part, axis, combine, identity):
@@ -82,7 +88,19 @@
         w_beta,
         w_decay,
     )
-    piece = lax.all_gather(tokens, "tp", axis=1, tiled=True)
+    size = lax.axis_size("tp")
+    pairs = [(i_2, (i_2 + 1) % size) for i_2 in range(size)]
+    back = [(b, a) for a, b in pairs]
+    lower_2, upper = ([], [])
+    for step in range(size - 1):
+        if step % 2 == 0:
+            lower_2.append(lax.ppermute(lower_2[-1] if lower_2 else tokens, "tp", pairs))
+        else:
+            upper.append(lax.ppermute(upper[-1] if upper else tokens, "tp", back))
+    tiles = jnp.stack([*lower_2[::-1], tokens, *upper])
+    shift = lax.axis_index("tp") - len(lower_2)
+    tiles = tiles[(jnp.arange(size) - shift) % size]
+    piece = laid_out(tiles, 1)
     totals = tuple(
         (jnp.dot(piece, weight, preferred_element_type=jnp.float32) for weight in weights)
     )

time: 488 us -> 508 us (1.041)
  local copies, waits for them, and re-layouts: 27.1 us -> 38.6 us
  starting transfers between devices: 3.58 us -> 10.2 us
    all_gather x1 -> x0, waiting for transfers between devices: 36.6 us -> none  [local(): piece = lax.all_gather(tokens, 'tp', axis=1, tiled=True)]
    ppermute x0 -> x3, waiting for transfers between devices: none -> 30.9 us  [the longest x2 30.9 us: local(): lax.ppermute(lower_2[-1] if lower_2 else tokens, 'tp', pairs)]
    transpose x0 -> x1, local copies, waits for them, and re-layouts: none -> 6.3 us  [laid_out(): return jnp.moveaxis(tiles, 0, dim).reshape(shape)]
  transfers between devices with their start and end apart: 4 -> 6, of which waited for: 3 -> 4; matrix products, arithmetic and copies ran while one was open for 3% -> 3% of each run, Pallas kernels for 0% -> 0%
where the time goes in v1:
time: 508 us; the launch traced here: 503 us
  other arithmetic  182 us (36%)
  matrix products  141 us (28%)
  waiting for transfers between devices  112 us (22%)
  local copies, waits for them, and re-layouts  38.6 us (8%)
  between operations  13.8 us (3%)
  starting transfers between devices  10.2 us (2%)
  blocking collectives  6.04 us (1%)
    another operation x4, other arithmetic, block_terms(): jax.scipy.linalg.solve_triangular(identity + lower, right, lower=True, un...  159 us
    reduce_scatter x1, waiting for transfers between devices, local(): lax.psum_scatter((summed + jnp.dot(conv_mixed, out_conv, preferred_elemen...  53.4 us
    ppermute x2, waiting for transfers between devices, local(): lax.ppermute(lower_2[-1] if lower_2 else tokens, 'tp', pairs)  30.9 us
    dot_general x16, matrix products, advance(): jnp.einsum('hcs,hse->hce', scores_block, fresh, precision=HIGHEST)  28.1 us
    all_gather x1, waiting for transfers between devices, entering(): gathered = lax.all_gather(part, axis)  27.6 us
    dot_general x16, matrix products, advance(): jnp.einsum('hcd,hce->hde', weighted, fresh, precision=HIGHEST)  21.5 us
    dot_general x7, matrix products, local(): jnp.dot(piece, weight, preferred_element_type=jnp.float32)  20.8 us
    dot_general x16, matrix products, advance(): jnp.einsum('hcd,hde->hce', query_block * jnp.exp(log_block)[..., None], m...  18.5 us
  transfers between devices with their start and end apart: 6, of which 4 were waited for; matrix products, arithmetic and copies ran while one was open for 3% of the time, Pallas kernels for 0%

profile of v1, /device:TPU:0, one launch (start us, length us, event | category | flops | bytes accessed | tf_op | source)
XLA Modules:
  0.0 503.3 jit_solution(6929417415715291817)
XLA Ops:
  9.0 21.3 %collective-permute-done = bf16[1024,512]{1,0:T(8,128)(2,1)S(1)} collective-permute-done((bf16[1024,512]{1,0:T(8,128)(2,1)}, bf16[1024,512]{1,0:T(8,128)(2,1)S(1)}, u32[]{:S(2)}, u32[]{:S(2)}) %collective-permute-start) | collective-permute-done | bytes 1048608 | tf_op jit(solution)/shard_map/ppermute | solution.py:97
  30.3 2.6 collective-permute-start.1
  35.1 9.5 %collective-permute-done.1 = bf16[1024,512]{1,0:T(8,128)(2,1)} collective-permute-done((bf16[1024,512]{1,0:T(8,128)(2,1)S(1)}, bf16[1024,512]{1,0:T(8,128)(2,1)}, u32[]{:S(2)}, u32[]{:S(2)}) %collective-permute-start.1) | collective-permute-done | bytes 1048608 | tf_op jit(solution)/shard_map/ppermute | solution.py:97
  44.6 3.4 pad_maximum_fusion
  48.0 5.0 gather_fusion
  53.0 3.1 multiply_reduce_fusion
  56.1 6.3 %copy.67 = bf16[1024,4,512]{0,2,1:T(8,128)(2,1)} copy(bf16[1024,4,512]{2,0,1:T(8,128)(2,1)} %bitcast.194) | data formatting | bytes 8388608 | tf_op jit(solution)/shard_map/transpose | solution.py:15
  62.5 3.0 fusion.147
  67.2 3.5 fusion.47
  71.6 3.8 fusion.45
  76.9 4.8 fusion.43
  84.5 3.7 fusion.39
  88.2 158.7 %custom-call.4 = f32[2,16,1,64,64]{3,4,2,1,0:T(8,128)} custom-call(f32[2,16,1,64,64]{4,3,2,1,0:T(8,128)} %fusion.39), custom_call_target="InvertDiagBlocksLowerTriangular" | custom-call | tf_op jit(solution)/shard_map/jit(_solve_triangular)/vmap(vmap())/triangular_solve | solution.py:50
  255.5 3.1 fusion.26
  258.6 104.3 %while.22 = (s32[]{:T(128)}, f32[2,128,256]{2,1,0:T(8,128)S(1)}, f32[16,2,64,256]{3,2,1,0:T(8,128)}, f32[16,2,64]{2,0,1:T(8,128)S(1)}, f32[16,2,64,128]{3,2,1,0:...) while((s32[]{:T(128)}, f32[2,128,256]{2,1,0:T(8,128)S(1)}, ...), condition=%wide.region_5.6_spmd, body=%wide.region_4.5_spmd.sunk | while | flops 176390272 | bytes 2298537 | solution.py:166
  363.8 3.8 fusion.58
  369.8 5.1 %collective-permute-start.3 = (bf16[30,256]{1,0:T(8,128)(2,1)S(1)}, bf16[30,256]{1,0:T(8,128)(2,1)S(1)}, u32[]{:S(2)}, u32[]{:S(2)}) collective-permute-start(bf16[30,256]{1,0:T(8,128)(2,1)S(1)} %slice.294), channel_id=1, source_target_pairs={{0,4},{4,8},{8,12},{12,16},{16,20},{20,24},{24,28},{1,5},{5,9},{9,... | collective-permute-start | bytes 46088 | tf_op jit(solution)/shard_map/ppermute | solution.py:32
  377.5 6.0 %fusion.144 = (f32[1024]{0:T(1024)S(1)}, f32[1024]{0:T(1024)S(1)}, f32[1024,256]{1,0:T(8,128)}) fusion(f32[256]{0:T(256)S(1)} %bitcast.237, bf16[1024,256]{1,0:T(8,128)(2,1)S(1)} %copy-done.10, f32[256]{0:T(256)S(1)} %bitcast.238, bf16[30,256]{1,0:T(8,128)(2,1)S(1)} %collective-permute-done.3, f32[256]{0:T(256)S(1)} %bitcast.209, f32[256]{0:T(256)S(1)} %bitcast.210, ...), kind=kLoop, calls=%fused_computation.261 | loop fusion | flops 48494592 | bytes 1628160 | tf_op jit(solution)/shard_map/reduce_sum | solution.py:202
  383.4 6.0 %all-reduce.3 = (f32[1024]{0:T(1024)S(1)}, f32[1024]{0:T(1024)S(1)}) all-reduce(f32[1024]{0:T(1024)S(1)} %get-tuple-element.118, f32[1024]{0:T(1024)S(1)} %get-tuple-element.117), channel_id=1, replica_groups=mesh['sp'=8,'tp'=4] {'tp'}, use_global_device_ids=true, to_apply=%region_12.13 | all-reduce | flops 2048 | bytes 16384 | tf_op jit(solution)/shard_map/psum | solution.py:204
  389.5 27.6 %all-gather.3.cloned.1.call-done = f32[16,128,256]{2,1,0:T(8,128)} async-done(((f32[2,128,256]{2,1,0:T(8,128)}), f32[16,128,256]{2,1,0:T(8,128)}) %all-gather.3.cloned.1.call-update) | async-done | bytes 2097168 | tf_op jit(solution)/shard_map/all_gather | solution.py:20
  417.9 2.9 multiply_reduce_fusion.2
  420.9 10.6 %fusion.65 = f32[1024,2048]{1,0:T(8,128)} fusion(bf16[256,2048]{1,0:T(8,128)(2,1)S(1)} %copy-done, bf16[1024,2048]{0,1:T(8,128)(2,1)} %bitcast.190, bf16[2048,256]{1,0:T(8,128)(2,1)} %param.25, f32[1024]{0:T(1024)S(1)} %add_rsqrt_fusion.4, f32[1024,2,128]{2,0,1:T(8,128)} %get-tuple-element.194, f32[128]{0:T(128)S(1)} %copy-done.28, ...), kind=kOutput, calls=%fused_computation.112 | convolution fusion | flops 2150367232 | bytes 15741440 | tf_op jit(solution)/shard_map/dot_general | solution.py:214
  431.5 11.5 %add_convert_fusion = bf16[1024,2048]{1,0:T(8,128)(2,1)} fusion(f32[1024,2048]{1,0:T(8,128)} %fusion.65, bf16[256,2048]{1,0:T(8,128)(2,1)S(1)} %copy-done.25, bf16[1024,2048]{0,1:T(8,128)(2,1)} %bitcast.191, bf16[2048,256]{1,0:T(8,128)(2,1)} %param.28, f32[1024,256]{1,0:T(8,128)S(1)} %copy-done.8, f32[256]{0:T(256)S(1)} %copy-done.26, ...), kind=kOutput, calls=%fused_computation.29 | convolution fusion | flops 2156134400 | bytes 19937280 | tf_op jit(solution)/shard_map/dot_general | solution.py:216
  443.1 53.4 %reduce-scatter.2.cloned.1.call-done = bf16[256,2048]{1,0:T(8,128)(2,1)} async-done(((bf16[1024,2048]{1,0:T(8,128)(2,1)}), bf16[256,2048]{1,0:T(8,128)(2,1)}) %reduce-scatter.2.cloned.1.call-update) | async-done | bytes 1048592 | tf_op jit(solution)/shard_map/reduce_scatter | solution.py:215
  (234 shorter events, 130.3 us)
Async XLA Ops:
  6.5 414.3 %copy-start = (bf16[256,2048]{1,0:T(8,128)(2,1)S(1)}, bf16[256,2048]{1,0:T(8,128)(2,1)}, u32[]{:S(2)}) copy-start(bf16[256,2048]{1,0:T(8,128)(2,1)} %param.36) | copy-start | bytes 3145732
  6.5 410.5 %all-gather.3.cloned.1.call-start = ((), (), s32[]{:S(2)}) async-start(), calls=%async_computation.2 | async-start | bytes 2359296 | tf_op jit(solution)/shard_map/all_gather | solution.py:20
  6.5 23.8 %collective-permute-start = (bf16[1024,512]{1,0:T(8,128)(2,1)}, bf16[1024,512]{1,0:T(8,128)(2,1)S(1)}, u32[]{:S(2)}, u32[]{:S(2)}) collective-permute-start(bf16[1024,512]{1,0:T(8,128)(2,1)} %param.21), channel_id=1, source_target_pairs={{0,1},{1,2},{2,3},{3,0},{4,5},{5,6},{6,7},{7,4},{8,9},{9,10},{10,1... | collective-permute-start | bytes 3145736 | tf_op jit(solution)/shard_map/ppermute | solution.py:97
  7.0 28.1 %collective-permute-start.2 = (bf16[1024,512]{1,0:T(8,128)(2,1)}, bf16[1024,512]{1,0:T(8,128)(2,1)S(1)}, u32[]{:S(2)}, u32[]{:S(2)}) collective-permute-start(bf16[1024,512]{1,0:T(8,128)(2,1)} %param.21), channel_id=1, source_target_pairs={{1,0},{2,1},{3,2},{0,3},{5,4},{6,5},{7,6},{4,7},{9,8},{10,9},{11,1... | collective-permute-start | bytes 3145736 | tf_op jit(solution)/shard_map/ppermute | solution.py:99
  30.3 14.3 %collective-permute-start.1 = (bf16[1024,512]{1,0:T(8,128)(2,1)S(1)}, bf16[1024,512]{1,0:T(8,128)(2,1)}, u32[]{:S(2)}, u32[]{:S(2)}) collective-permute-start(bf16[1024,512]{1,0:T(8,128)(2,1)S(1)} %collective-permute-done), channel_id=1, source_target_pairs={{0,1},{1,2},{2,3},{3,0},{4,5},{5,6},{6,7},{7,4},{8,9},{9,10},{10,1... | collective-permute-start | bytes 3145736 | tf_op jit(solution)/shard_map/ppermute | solution.py:97
  33.0 29.4 %copy-start.1 = (f32[2,128,256]{2,1,0:T(8,128)}, f32[2,128,256]{2,1,0:T(8,128)S(1)}, u32[]{:S(2)}) copy-start(f32[2,128,256]{2,1,0:T(8,128)S(1)} %concatenate.15) | copy-start | bytes 786436
  56.1 6.3 %copy-start.12 = (bf16[2048,8]{0,1:T(8,128)(2,1)S(1)}, bf16[2048,8]{0,1:T(8,128)(2,1)}, u32[]{:S(2)}) copy-start(bf16[2048,8]{0,1:T(8,128)(2,1)} %param.29) | copy-start | bytes 98308
  62.4 4.8 copy-start.22
  76.9 7.5 %copy-start.14 = (f32[64,64]{1,0:T(8,128)S(1)}, f32[64,64]{1,0:T(8,128)}, u32[]{:S(2)}) copy-start(f32[64,64]{1,0:T(8,128)} %get-tuple-element.198) | copy-start | bytes 49156
  76.9 7.5 %copy-start.16 = (pred[64,64]{1,0:T(8,128)(4,1)S(1)}, pred[64,64]{1,0:T(8,128)(4,1)}, u32[]{:S(2)}) copy-start(pred[64,64]{1,0:T(8,128)(4,1)} %get-tuple-element.196) | copy-start | bytes 12292
  76.9 7.5 %copy-start.17 = (pred[64,64]{1,0:T(8,128)(4,1)S(1)}, pred[64,64]{1,0:T(8,128)(4,1)}, u32[]{:S(2)}) copy-start(pred[64,64]{1,0:T(8,128)(4,1)} %get-tuple-element.197) | copy-start | bytes 12292
  251.2 4.3 copy-start.15
  252.9 5.8 %copy-start.4 = (f32[2,128,256]{2,1,0:T(8,128)S(1)}, f32[2,128,256]{2,1,0:T(8,128)}, u32[]{:S(2)}) copy-start(f32[2,128,256]{2,1,0:T(8,128)} %copy-done.1) | copy-start | bytes 786436
  258.6 105.1 %copy-start.11 = (bf16[31,256]{1,0:T(8,128)(2,1)S(1)}, bf16[31,256]{1,0:T(8,128)(2,1)}, u32[]{:S(2)}) copy-start(bf16[31,256]{1,0:T(8,128)(2,1)} %param.33) | copy-start | bytes 47620
  258.6 105.1 %copy-start.23 = (bf16[2048,256]{1,0:T(8,128)(2,1)S(1)}, bf16[2048,256]{1,0:T(8,128)(2,1)}, u32[]{:S(2)}) copy-start(bf16[2048,256]{1,0:T(8,128)(2,1)} %param.27) | copy-start | bytes 3145732
  363.7 132.8 %reduce-scatter.2.cloned.1.call-start = ((), (), s32[]{:S(2)}) async-start(), calls=%async_computation.1 | async-start | bytes 5242880 | tf_op jit(solution)/shard_map/reduce_scatter | solution.py:215
  363.8 3.8 copy-start.6
  363.8 3.8 copy-start.24
  369.8 47.3 %copy-start.2 = (f32[2,128,256]{2,1,0:T(8,128)S(1)}, f32[2,128,256]{2,1,0:T(8,128)}, u32[]{:S(2)}) copy-start(f32[2,128,256]{2,1,0:T(8,128)} %copy-done.1) | copy-start | bytes 786436
  369.8 7.7 %collective-permute-start.3 = (bf16[30,256]{1,0:T(8,128)(2,1)S(1)}, bf16[30,256]{1,0:T(8,128)(2,1)S(1)}, u32[]{:S(2)}, u32[]{:S(2)}) collective-permute-start(bf16[30,256]{1,0:T(8,128)(2,1)S(1)} %slice.294), channel_id=1, source_target_pairs={{0,4},{4,8},{8,12},{12,16},{16,20},{20,24},{24,28},{1,5},{5,9},{9,... | collective-permute-start | bytes 46088 | tf_op jit(solution)/shard_map/ppermute | solution.py:32
  420.9 10.7 %copy-start.8 = (f32[1024,256]{1,0:T(8,128)S(1)}, f32[1024,256]{1,0:T(8,128)}, u32[]{:S(2)}) copy-start(f32[1024,256]{1,0:T(8,128)} %get-tuple-element.147) | copy-start | bytes 3145732
  420.9 10.6 %copy-start.25 = (bf16[256,2048]{1,0:T(8,128)(2,1)S(1)}, bf16[256,2048]{1,0:T(8,128)(2,1)}, u32[]{:S(2)}) copy-start(bf16[256,2048]{1,0:T(8,128)(2,1)} %param.37) | copy-start | bytes 3145732
  420.9 10.6 %copy-start.26 = (f32[256]{0:T(256)S(1)}, f32[256]{0:T(256)}, u32[]{:S(2)}) copy-start(f32[256]{0:T(256)} %param.35) | copy-start | bytes 3076
  420.9 10.6 %copy-start.27 = (f32[256]{0:T(256)S(1)}, f32[256]{0:T(256)}, u32[]{:S(2)}) copy-start(f32[256]{0:T(256)} %param.34) | copy-start | bytes 3076
  (11 other events, 24.2 us)
Sparse Core Ops, SparseCore 0:
  363.8 53.2 all-gather.2
  443.2 53.2 reduce-scatter.1
